TPU v7x, 32 devices: a whole 2x2x4 slice. The times are simulated.
32 devices in a mesh: grp: 2 (over y), ep: 4 (over z), tp: 4 (over x, core).
Axes of the slice: x: 2, y: 2, z: 4, core: 2. Of those that a mesh axis runs over, the one named last changes fastest.
Arguments:
- conv_input: bfloat16 [5120, 2048], P(('grp', 'ep')), parts along dimension 0, may hold values from -6 to 6
- conv_taps: float32 [31, 2048], replicated, may hold values from -1 to 1
- conv_gain: float32 [2048], replicated, may hold values from 0.1 to 1.9
- conv_weight: bfloat16 [2048, 2048], P(None, 'tp'), may hold values from -0.125 to 0.125
- moe_input: bfloat16 [5120, 2048], P(('grp', 'ep')), parts along dimension 0, may hold values from -6 to 6
- moe_gain: float32 [2048], replicated, may hold values from 0.1 to 1.9
- expert_ids: int32 [5120, 2], P(('grp', 'ep')), parts along dimension 0, may hold values from 0 to 3, as said below
- route_weights: float32 [5120, 2], P(('grp', 'ep')), parts along dimension 0, may hold values from 0.1 to 1
- gate_weight: bfloat16 [4, 2048, 1024], P('ep', None, 'tp'), may hold values from -0.125 to 0.125
- up_weight: bfloat16 [4, 2048, 1024], P('ep', None, 'tp'), may hold values from -0.125 to 0.125
- down_weight: bfloat16 [4, 1024, 2048], P('ep', 'tp'), may hold values from -0.1875 to 0.1875
- post_gain: float32 [2048], replicated, may hold values from 0.1 to 1.9
Outputs:
- conv_out: bfloat16 [5120, 2048], P(('grp', 'ep'), 'tp'), parts along dimension 0
- moe_out: bfloat16 [5120, 2048], P(('grp', 'ep', 'tp')), parts along dimension 0
There are 2 independent parts, one for each index of `grp`. A program takes and returns all parts, laid end to end along the dimension named above; an argument that names none is the same for every part. Nothing has to cross between parts.
Inputs may be any that keep to these rules, and one draw needn't show every extreme that they name: `expert_ids`: in each aligned block of 160 tokens, every expert is named exactly 80 times; a token's two experts differ and lie in one group of 4 consecutive experts.
All inputs are finite; a program needn't handle non-finite values.
Results may differ from a plain program's by a relative error of at most 0.012.
Values may be sent and summed in bfloat16 or wider, within the bound.
A program may use at most 128 MiB of HBM per device.

v0:
```python
import jax
import jax.numpy as jnp
from jax import lax
from jax.sharding import PartitionSpec as P

EPSILON = 1e-06


def shifted(shard, axis, by):
    size = lax.axis_size(axis)
    pairs = [(i, i + by) for i in range(size) if 0 <= i + by < size]
    return lax.ppermute(shard, axis, pairs)


def channel_norm(values, scales):
    mean_square = jnp.mean(values * values, axis=-1, keepdims=True)
    return values * lax.rsqrt(mean_square + EPSILON) * scales


def body(
    conv_input,
    conv_taps,
    conv_gain,
    conv_weight,
    moe_input,
    moe_gain,
    expert_ids,
    route_weights,
    gate_weight,
    up_weight,
    down_weight,
    post_gain,
):
    row_count = conv_input.shape[0]
    reach = conv_taps.shape[0] - 1
    carried = shifted(conv_input[row_count - reach :], "ep", 1)
    extended = jnp.concatenate([carried, conv_input], axis=0).astype(jnp.float32)
    conv_sum = extended[0:row_count] * conv_taps[0]
    for offset in range(1, reach + 1):
        conv_sum = conv_sum + extended[offset : offset + row_count] * conv_taps[offset]
    activated = jax.nn.silu(channel_norm(conv_sum, conv_gain)).astype(jnp.bfloat16)
    conv_out = jnp.dot(activated, conv_weight, preferred_element_type=jnp.float32).astype(
        jnp.bfloat16
    )
    model_width = moe_input.shape[1]
    quarters = lax.axis_size("tp")
    ep_count = lax.axis_size("ep")
    block_rows = moe_input.shape[0] // quarters
    local_experts = gate_weight.shape[0]
    experts_all = ep_count * local_experts
    capacity = 2 * block_rows // experts_all
    slot_rows = 2 * block_rows
    own_quarter = lax.axis_index("tp")
    entries = expert_ids.reshape(quarters, slot_rows)
    onehot = (
        entries[:, :, None] == jnp.arange(experts_all, dtype=jnp.int32)[None, None, :]
    ).astype(jnp.int32)
    position = jnp.sum((jnp.cumsum(onehot, axis=1) - 1) * onehot, axis=2)
    target = entries * capacity + position
    quarter_index = jnp.arange(quarters, dtype=jnp.int32)[:, None]
    entry_index = jnp.broadcast_to(
        jnp.arange(slot_rows, dtype=jnp.int32)[None, :], (quarters, slot_rows)
    )
    source_entry = (
        jnp.zeros((quarters, slot_rows), jnp.int32).at[quarter_index, target].set(entry_index)
    )
    own_input = lax.dynamic_slice_in_dim(moe_input, own_quarter * block_rows, block_rows, 0)
    normed = channel_norm(own_input.astype(jnp.float32), moe_gain).astype(jnp.bfloat16)
    own_source = lax.dynamic_index_in_dim(source_entry, own_quarter, 0, keepdims=False)
    arrived = lax.all_to_all(
        normed[own_source // 2].reshape(1, ep_count, local_experts * capacity, model_width),
        "ep",
        split_axis=1,
        concat_axis=1,
        tiled=True,
    )
    gate_full, up_full, down_full = (
        lax.all_gather(gate_weight, "tp", axis=2, tiled=True),
        lax.all_gather(up_weight, "tp", axis=2, tiled=True),
        lax.all_gather(down_weight, "tp", axis=1, tiled=True),
    )
    count = arrived.shape[0]
    shaped = arrived.reshape(count, ep_count, local_experts, capacity, model_width)
    gate_value = jnp.einsum(
        "qsjcd,jdf->qsjcf", shaped, gate_full, preferred_element_type=jnp.float32
    )
    up_value = jnp.einsum("qsjcd,jdf->qsjcf", shaped, up_full, preferred_element_type=jnp.float32)
    hidden = (jax.nn.silu(gate_value) * up_value).astype(jnp.bfloat16)
    hidden_units = down_full.shape[1]
    part_units = hidden_units // quarters
    pieces = hidden.reshape(ep_count, local_experts, capacity, quarters, part_units)
    down_pieces = down_full.reshape(local_experts, quarters, part_units, model_width)
    partial_value = jnp.einsum(
        "sjctf,jtfd->sjctd", pieces, down_pieces, preferred_element_type=jnp.float32
    )
    summed = jnp.sum(partial_value.astype(jnp.bfloat16).astype(jnp.float32), axis=3).astype(
        jnp.bfloat16
    )
    summed = summed.reshape(slot_rows, model_width)
    returned = lax.all_to_all(
        summed.reshape(ep_count, local_experts * capacity, model_width),
        "ep",
        split_axis=0,
        concat_axis=0,
        tiled=True,
    )
    flat_back = returned.reshape(slot_rows, model_width)
    own_target = lax.dynamic_index_in_dim(target, own_quarter, 0, keepdims=False)
    gathered = flat_back[own_target].reshape(block_rows, 2, model_width).astype(jnp.float32)
    weights = lax.dynamic_slice_in_dim(route_weights, own_quarter * block_rows, block_rows, 0)
    mixed_rows = jnp.sum(gathered * weights[:, :, None], axis=1)
    moe_out = channel_norm(mixed_rows, post_gain).astype(jnp.bfloat16)
    return (conv_out, moe_out)


def solution(mesh):
    in_specs = (
        P(("grp", "ep"), None),
        P(),
        P(),
        P(None, "tp"),
        P(("grp", "ep"), None),
        P(),
        P(("grp", "ep"), None),
        P(("grp", "ep"), None),
        P("ep", None, "tp"),
        P("ep", None, "tp"),
        P("ep", "tp", None),
        P(),
    )
    out_specs = (P(("grp", "ep"), "tp"), P(("grp", "ep", "tp"), None))
    return jax.shard_map(body, mesh=mesh, in_specs=in_specs, out_specs=out_specs, check_vma=False)
```

profile of v0, /device:TPU:0, one launch (start us, length us, event | category | flops | bytes accessed | tf_op | source)
XLA Modules:
  0.0 225.6 jit_solution(16062887784778306513)
XLA Ops:
  7.2 0.7 all-gather.4.cloned.1.call-update
  8.0 0.7 all-gather.6.cloned.1.call-update
  8.7 0.7 all-gather.8.cloned.1.call-update
  9.4 0.9 copy.26
  10.3 0.2 eq.22
  10.5 4.8 %reduce-window.6 = s32[4,4,3,128]{3,2,1,0:T(4,128)S(1)} reduce-window(s32[4,4,3,128]{3,2,1,0:T(4,128)S(1)} %copy.27, s32[]{:T(128)} %constant.58.clone.1), window={size=1x1x1x128 pad=0_0x0_0x0_0x127_0}, to_apply=%region_2.3 | reduce-window | flops 780288 | bytes 49156 | tf_op jit(solution)/shard_map/reduce-window
  15.4 0.1 slice.299
  15.5 0.2 copy.28
  15.6 0.1 copy.29
  15.8 0.1 broadcast_add_fusion
  15.9 0.7 broadcast_multiply_fusion
  16.6 0.2 copy.25
  16.7 0.2 mul.520
  17.0 0.7 multiply_reduce_fusion.3
  17.8 0.7 and_reduce_fusion
  18.5 0.1 reshape.251
  18.6 0.1 reshape.253
  18.7 5.2 %scatter_custom_fusion = s32[1280]{0:T(1024)S(1)} fusion(s32[1280]{0:T(1024)S(1)} %reshape.251, s32[1280]{0:T(1024)S(1)} %reshape.253, s32[]{:T(128)} %constant.58.clone.1), kind=kCustom, calls=%fused_computation.108 | custom fusion | bytes 5124
  24.0 0.1 reshape.232
  24.1 1.3 fusion.48
  25.4 1.3 fusion.50
  26.7 3.0 %gather_fusion = bf16[320,2048]{1,0:T(8,128)(2,1)} fusion(bf16[160,2048]{1,0:T(8,128)(2,1)S(1)} %fusion.50, s32[1024]{0:T(1024)S(1)} %pad_clamp_fusion.1), kind=kCustom, calls=%fused_computation | custom fusion | bytes 2622720 | tf_op jit(solution)/shard_map/gather | solution.py:71
  29.8 6.3 %all-to-all-start = ((bf16[1,4,80,2048]{3,2,0,1:T(8,128)(2,1)}), bf16[1,4,80,2048]{3,2,0,1:T(8,128)(2,1)S(1)}, u32[]{:S(2)}, u32[]{:S(2)}) async-start(bf16[1,4,80,2048]{3,2,0,1:T(8,128)(2,1)} %bitcast.108), calls=%async_computation | async-start | bytes 2621440 | tf_op jit(solution)/shard_map/all_to_all | solution.py:70
  36.1 1.6 slice.198
  37.7 4.6 %collective-permute-start = (bf16[30,2048]{1,0:T(8,128)(2,1)}, bf16[30,2048]{1,0:T(8,128)(2,1)}, u32[]{:S(2)}, u32[]{:S(2)}) collective-permute-start(bf16[30,2048]{1,0:T(8,128)(2,1)} %slice.198), channel_id=1, source_target_pairs={{0,4},{4,8},{8,12},{1,5},{5,9},{9,13},{2,6},{6,10},{10,14},{3,7},{... | collective-permute-start | bytes 368648 | tf_op jit(solution)/shard_map/ppermute | solution.py:12
  42.3 2.0 fusion.66
  44.3 2.4 %fusion.65 = (f32[1,2048]{1,0:T(1,128)}, f32[1,2048]{1,0:T(1,128)}, f32[1,2048]{1,0:T(1,128)}, f32[1,2048]{1,0:T(1,128)}, f32[1,2048]{1,0:T(1,128)}, /*index=5*/...) fusion(f32[31,2048]{1,0:T(8,128)} %param.13), kind=kLoop, calls=%fused_computation.126 | loop fusion | bytes 311296 | tf_op jit(solution)/shard_map/slice | solution.py:38
  46.6 1.4 constant_dynamic-slice_fusion
  48.0 0.8 copy.32
  48.8 0.7 fusion.61
  49.5 0.6 pad_clamp_fusion
  50.1 10.2 %collective-permute-done = bf16[30,2048]{1,0:T(8,128)(2,1)} collective-permute-done((bf16[30,2048]{1,0:T(8,128)(2,1)}, bf16[30,2048]{1,0:T(8,128)(2,1)}, u32[]{:S(2)}, u32[]{:S(2)}) %collective-permute-start) | collective-permute-done | bytes 122912 | tf_op jit(solution)/shard_map/ppermute | solution.py:12
  60.3 5.0 %maximum_convert_fusion = f32[670,2048]{1,0:T(8,128)} fusion(bf16[640,2048]{1,0:T(8,128)(2,1)} %param.12, bf16[30,2048]{1,0:T(8,128)(2,1)} %collective-permute-done), kind=kLoop, calls=%fused_computation.71 | loop fusion | flops 5488640 | bytes 8232960 | tf_op jit(solution)/shard_map/convert_element_type | solution.py:37
  65.3 2.2 all-to-all-done
  67.5 4.8 %fusion.35 = f32[1,4,1,80,1024]{4,3,1,0,2:T(8,128)} fusion(bf16[1,2048,1024]{2,1,0:T(8,128)(2,1)} %all-gather.4.cloned.1.call-done, bf16[1,4,80,2048]{3,2,0,1:T(8,128)(2,1)S(1)} %all-to-all-done), kind=kOutput, calls=%fused_computation.76 | convolution fusion | flops 1342177280 | bytes 6815744 | tf_op jit(solution)/shard_map/qsjcd,jdf->qsjcf/dot_general | solution.py:84
  72.2 11.6 %all-gather.6.cloned.1.call-done = bf16[1,2048,1024]{2,1,0:T(8,128)(2,1)} async-done(((bf16[1,2048,256]{2,1,0:T(8,128)(2,1)}), bf16[1,2048,1024]{2,1,0:T(8,128)(2,1)}) %all-gather.6.cloned.1.call-update) | async-done | bytes 4194320 | tf_op jit(solution)/shard_map/all_gather | solution.py:79
  83.9 5.0 %fusion.44 = bf16[1,4,1,80,1024]{4,3,1,0,2:T(8,128)(2,1)} fusion(bf16[1,2048,1024]{2,1,0:T(8,128)(2,1)} %all-gather.6.cloned.1.call-done, bf16[1,4,80,2048]{3,2,0,1:T(8,128)(2,1)S(1)} %all-to-all-done, f32[1,4,1,80,1024]{4,3,1,0,2:T(8,128)} %fusion.35), kind=kOutput, calls=%fused_computation.79 | convolution fusion | flops 1344143360 | bytes 7471104 | tf_op jit(solution)/shard_map/qsjcd,jdf->qsjcf/dot_general | solution.py:87
  88.9 1.8 reshape.226
  90.7 29.2 %all-gather.8.cloned.1.call-done = bf16[1,1024,2048]{2,1,0:T(8,128)(2,1)} async-done(((bf16[1,256,2048]{2,1,0:T(8,128)(2,1)}), bf16[1,1024,2048]{2,1,0:T(8,128)(2,1)}) %all-gather.8.cloned.1.call-update) | async-done | bytes 4194320 | tf_op jit(solution)/shard_map/all_gather | solution.py:80
  119.9 5.1 %convert_reduce_fusion = bf16[4,80,2048]{2,1,0:T(8,128)(2,1)} fusion(bf16[4,256,2048,1]{2,1,3,0:T(8,128)(2,1)} %bitcast.141, bf16[4,80,4,256]{3,2,1,0:T(4,128)(2,1)S(1)} %reshape.226), kind=kOutput, calls=%fused_computation.64 | convolution fusion | flops 1346764800 | bytes 6160384 | tf_op jit(solution)/shard_map/sjctf,jtfd->sjctd/dot_general | solution.py:93
  125.1 4.6 %all-to-all-start.1 = ((bf16[4,80,2048]{2,1,0:T(8,128)(2,1)}), bf16[4,80,2048]{2,1,0:T(8,128)(2,1)S(1)}, u32[]{:S(2)}, u32[]{:S(2)}) async-start(bf16[4,80,2048]{2,1,0:T(8,128)(2,1)} %convert_reduce_fusion), calls=%async_computation.1 | async-start | bytes 2621440 | tf_op jit(solution)/shard_map/all_to_all | solution.py:100
  129.7 72.7 %multiply_reduce_fusion = (f32[640]{0:T(1024)S(1)}, f32[640,2048]{1,0:T(8,128)S(1)}) fusion(f32[2048]{0:T(1024)} %bitcast.120, f32[670,2048]{1,0:T(8,128)} %maximum_convert_fusion, f32[2048]{0:T(1024)} %bitcast.121, f32[2048]{0:T(1024)} %bitcast.123, f32[2048]{0:T(1024)} %bitcast.124, f32[2048]{0:T(1024)} %bitcast.125, f32[2048]{0:T(1024)} %bitcast.126, ...), kind=kLoop, calls=%fused_computation.66 | loop fusion | flops 82574720 | bytes 168028672 | tf_op jit(solution)/shard_map/reduce_sum | solution.py:16
  202.5 2.5 %fusion.47 = bf16[640,512]{1,0:T(8,128)(2,1)} fusion(bf16[2048,512]{1,0:T(8,128)(2,1)S(1)} %copy-done, f32[640,2048]{1,0:T(8,128)S(1)} %get-tuple-element.3, f32[2048]{0:T(1024)S(1)} %copy-done.6, f32[640]{0:T(1024)S(1)} %add_rsqrt_fusion), kind=kOutput, calls=%fused_computation.80 | convolution fusion | flops 1351680000 | bytes 8006144 | tf_op jit(solution)/shard_map/dot_general | solution.py:42
  205.0 3.0 %gather_fusion.1 = bf16[320,2048]{1,0:T(8,128)(2,1)} fusion(bf16[320,2048]{1,0:T(8,128)(2,1)S(1)} %bitcast.107, s32[1024]{0:T(1024)S(1)} %copy-done.3), kind=kCustom, calls=%fused_computation.1 | custom fusion | bytes 2622720 | tf_op jit(solution)/shard_map/gather | solution.py:109
  208.0 4.1 %reshape.234 = f32[160,2,2048]{2,1,0:T(2,128)} reshape(bf16[320,2048]{1,0:T(8,128)(2,1)} %gather_fusion.1) | data formatting | bytes 3932160 | tf_op jit(solution)/shard_map/convert_element_type | solution.py:109
  212.1 5.8 %multiply_reduce_fusion.1 = f32[160,2048]{1,0:T(8,128)S(1)} fusion(f32[160,2,2048]{2,1,0:T(2,128)} %reshape.234, f32[160,2]{1,0:T(8,128)S(1)} %copy.32), kind=kLoop, calls=%fused_computation.72 | loop fusion | flops 983040 | bytes 3933440 | tf_op jit(solution)/shard_map/reduce_sum | solution.py:111
  217.9 0.2 multiply_reduce_fusion.2
  218.1 1.0 multiply_convert_fusion.4
  (35 shorter events, 0.3 us)
Async XLA Ops:
  7.2 195.3 %copy-start = (bf16[2048,512]{1,0:T(8,128)(2,1)S(1)}, bf16[2048,512]{1,0:T(8,128)(2,1)}, u32[]{:S(2)}) copy-start(bf16[2048,512]{1,0:T(8,128)(2,1)} %param.15) | copy-start | bytes 6291460
  7.2 18.2 %copy-start.4 = (f32[2048]{0:T(1024)S(1)}, f32[2048]{0:T(1024)}, u32[]{:S(2)}) copy-start(f32[2048]{0:T(1024)} %param.17) | copy-start | bytes 24580
  7.2 60.3 %all-gather.4.cloned.1.call-start = ((), (), s32[]{:S(2)}) async-start(), calls=%async_computation.2 | async-start | bytes 5242880 | tf_op jit(solution)/shard_map/all_gather | solution.py:78
  7.9 76.0 %all-gather.6.cloned.1.call-start = ((), (), s32[]{:S(2)}) async-start(), calls=%async_computation.3 | async-start | bytes 5242880 | tf_op jit(solution)/shard_map/all_gather | solution.py:79
  8.7 111.3 %all-gather.8.cloned.1.call-start = ((), (), s32[]{:S(2)}) async-start(), calls=%async_computation.4 | async-start | bytes 5242880 | tf_op jit(solution)/shard_map/all_gather | solution.py:80
  17.0 8.4 %copy-start.2 = (s32[4,320]{1,0:T(4,128)}, s32[4,320]{1,0:T(4,128)S(1)}, u32[]{:S(2)}) copy-start(s32[4,320]{1,0:T(4,128)S(1)} %fusion.55) | copy-start | bytes 15364
  29.8 37.7 %all-to-all-start = ((bf16[1,4,80,2048]{3,2,0,1:T(8,128)(2,1)}), bf16[1,4,80,2048]{3,2,0,1:T(8,128)(2,1)S(1)}, u32[]{:S(2)}, u32[]{:S(2)}) async-start(bf16[1,4,80,2048]{3,2,0,1:T(8,128)(2,1)} %bitcast.108), calls=%async_computation | async-start | bytes 2621440 | tf_op jit(solution)/shard_map/all_to_all | solution.py:70
  37.7 22.6 %collective-permute-start = (bf16[30,2048]{1,0:T(8,128)(2,1)}, bf16[30,2048]{1,0:T(8,128)(2,1)}, u32[]{:S(2)}, u32[]{:S(2)}) collective-permute-start(bf16[30,2048]{1,0:T(8,128)(2,1)} %slice.198), channel_id=1, source_target_pairs={{0,4},{4,8},{8,12},{1,5},{5,9},{9,13},{2,6},{6,10},{10,14},{3,7},{... | collective-permute-start | bytes 368648 | tf_op jit(solution)/shard_map/ppermute | solution.py:12
  90.7 38.9 %copy-start.1 = (f32[1,2048]{1,0:T(1,128)S(1)}, f32[1,2048]{1,0:T(1,128)}, u32[]{:S(2)}) copy-start(f32[1,2048]{1,0:T(1,128)} %get-tuple-element.30) | copy-start | bytes 24580
  125.1 79.9 %all-to-all-start.1 = ((bf16[4,80,2048]{2,1,0:T(8,128)(2,1)}), bf16[4,80,2048]{2,1,0:T(8,128)(2,1)S(1)}, u32[]{:S(2)}, u32[]{:S(2)}) async-start(bf16[4,80,2048]{2,1,0:T(8,128)(2,1)} %convert_reduce_fusion), calls=%async_computation.1 | async-start | bytes 2621440 | tf_op jit(solution)/shard_map/all_to_all | solution.py:100
  129.7 72.8 %copy-start.6 = (f32[2048]{0:T(1024)S(1)}, f32[2048]{0:T(1024)}, u32[]{:S(2)}) copy-start(f32[2048]{0:T(1024)} %param.14) | copy-start | bytes 24580
  202.5 2.5 %copy-start.3 = (s32[1024]{0:T(1024)S(1)}, s32[1024]{0:T(1024)}, u32[]{:S(2)}) copy-start(s32[1024]{0:T(1024)} %pad_clamp_fusion) | copy-start | bytes 12292
  208.0 10.1 %copy-start.5 = (f32[2048]{0:T(1024)S(1)}, f32[2048]{0:T(1024)}, u32[]{:S(2)}) copy-start(f32[2048]{0:T(1024)} %param.23) | copy-start | bytes 24580
Sparse Core Ops, SparseCore 0:
  9.5 37.7 all-gather.3
  48.9 34.9 all-gather.5
  85.5 34.4 all-gather.7
where the time goes:
time: 227 us; the launch traced here: 226 us
  other arithmetic  96 us (42%)
  waiting for transfers between devices  55.3 us (24%)
  local copies, waits for them, and re-layouts  27.4 us (12%)
  matrix products  17.4 us (8%)
  starting transfers between devices  15.6 us (7%)
  between operations  14 us (6%)
    reduce_sum x3, other arithmetic, channel_norm(): mean_square = jnp.mean(values * values, axis=-1, keepdims=True)  74.2 us
    all_gather x1, waiting for transfers between devices, body(): lax.all_gather(down_weight, 'tp', axis=1, tiled=True)  29.2 us
    all_gather x1, waiting for transfers between devices, body(): lax.all_gather(up_weight, 'tp', axis=2, tiled=True)  11.6 us
    ppermute x1, waiting for transfers between devices, shifted(): return lax.ppermute(shard, axis, pairs)  10.2 us
    all_to_all x1, starting transfers between devices, body(): lax.all_to_all(normed[own_source // 2].reshape(1, ep_count, local_experts...  6.34 us
    unnamed x17, local copies, waits for them, and re-layouts  6.22 us
    reduce_sum x1, other arithmetic, body(): mixed_rows = jnp.sum(gathered * weights[:, :, None], axis=1)  5.82 us
    dot_general x1, matrix products, body(): jnp.einsum('sjctf,jtfd->sjctd', pieces, down_pieces, preferred_element_ty...  5.12 us
  transfers between devices with their start and end apart: 6, of which 4 were waited for; matrix products, arithmetic and copies ran while one was open for 54% of the time, Pallas kernels for 0%

commit v1 on v0

v1 whole, which is shorter than its diff:
```python
import functools

import jax
import jax.numpy as jnp
from jax import lax
from jax.experimental import pallas as pl
from jax.experimental.pallas import tpu as pltpu
from jax.sharding import PartitionSpec as P

EPSILON = 1e-06
MESH = pl.DeviceIdType.MESH
F32, BF16 = jnp.float32, jnp.bfloat16
CONV_ROWS = 64
LANES = 128


def silu(v):
    return v / (1.0 + jnp.exp(-v))


def kernel(
    sizes,
    conv_hbm,
    taps,
    conv_gain,
    convw_hbm,
    moe_hbm,
    moe_gain,
    ids_ref,
    route_ref,
    gate_hbm,
    up_hbm,
    down_hbm,
    post_gain,
    conv_out,
    moe_out,
    ext,
    convw,
    act,
    conv_sum,
    own_in,
    gate,
    up,
    down,
    mix,
    send_rows,
    got_rows,
    gate_val,
    hidden,
    result,
    back,
    sem_local,
    sem_halo,
    sem_a,
    sem_b,
    sem_c,
    sem_d,
    sem_e,
    sem_x,
    sem_y,
):
    groups, eps, tps = sizes
    highs = tps // 2
    g, e, t = lax.axis_index("grp"), lax.axis_index("ep"), lax.axis_index("tp")
    hi, lo = t // 2, t % 2
    partner = hi * 2 + (1 - lo)
    rows = conv_hbm.shape[0]
    width = conv_hbm.shape[1]
    reach = taps.shape[0] - 1
    halo = ext.shape[0] - rows
    block = own_in.shape[0]
    slots = 2 * block
    cap = slots // eps
    units = gate.shape[2]

    local = [
        pltpu.make_async_copy(
            moe_hbm.at[pl.ds(pl.multiple_of(t * block, 16), block)], own_in, sem_local.at[0]
        ),
        pltpu.make_async_copy(conv_hbm, ext.at[pl.ds(halo, rows)], sem_local.at[1]),
        pltpu.make_async_copy(convw_hbm, convw, sem_local.at[2]),
        pltpu.make_async_copy(gate_hbm.at[0], gate.at[t], sem_local.at[3]),
        pltpu.make_async_copy(up_hbm.at[0], up.at[t], sem_local.at[4]),
        pltpu.make_async_copy(down_hbm.at[0], down.at[t], sem_local.at[5]),
    ]
    for copy in local:
        copy.start()

    barrier = pltpu.get_barrier_semaphore()
    greet = [{"tp": partner}]
    greet += [{"tp": (hi + dh) % highs * 2 + lo} for dh in range(1, highs)]
    greet += [{"grp": (g + dg) % groups} for dg in range(1, groups)]
    greet += [{"ep": (e + de) % eps} for de in range(1, eps)]
    for other in greet:
        pl.semaphore_signal(barrier, inc=1, device_id=other, device_id_type=MESH)
    pl.semaphore_wait(barrier, len(greet))

    def remote(src, dst, sems, index, device):
        return pltpu.make_async_remote_copy(
            src_ref=src,
            dst_ref=dst,
            send_sem=sems.at[(0,) + index],
            recv_sem=sems.at[(1,) + index],
            device_id=device,
            device_id_type=MESH,
        )

    items = []
    half = width // 2
    for source, buffer in ((gate_hbm, gate), (up_hbm, up)):
        for part in range(2):
            items.append((source, buffer, part * half, half, 0, units))
    for part in range(2):
        items.append((down_hbm, down, 0, units, part * half, half))

    def view(ref, item, piece=None):
        _, _, r0, count, c0, columns = item
        if piece is None:
            return ref.at[pl.ds(r0, count), pl.ds(c0, columns)]
        size = count // groups
        start = pl.multiple_of(r0 + piece * size, 16)
        return ref.at[pl.ds(start, size), pl.ds(c0, columns)]

    def copy_a(i):
        item = items[i]
        return remote(
            view(item[0].at[0], item), view(item[1].at[t], item), sem_a, (i,), {"tp": partner}
        )

    def copy_b(i, dh):
        item = items[i]
        other = (hi + dh) % highs * 2 + lo
        return remote(
            view(item[0].at[0], item, g), view(item[1].at[t], item, g), sem_b, (i, dh), {"tp": other}
        )

    def origin(dh):
        return (hi + highs - dh) % highs * 2 + lo

    def copy_c(i, dh, dg):
        item = items[i]
        ref = view(item[1].at[origin(dh)], item, g)
        return remote(ref, ref, sem_c, (i, dh, dg), {"grp": (g + dg) % groups})

    def copy_d(i, dh):
        item = items[i]
        ref = view(item[1].at[origin(dh)], item, g)
        return remote(ref, ref, sem_d, (i, dh), {"tp": partner})

    def copy_e(i, dh, dg):
        item = items[i]
        ref = view(item[1].at[origin(dh)], item, (g + groups - dg) % groups)
        return remote(ref, ref, sem_e, (i, dh, dg), {"tp": partner})

    count = len(items)
    for i in range(count):
        for dh in range(1, highs):
            copy_b(i, dh).start()
    for i in range(count):
        copy_a(i).start()

    def relay_cross(i):
        for dh in range(1, highs):
            copy_b(i, dh).wait_recv()
            for dg in range(1, groups):
                copy_c(i, dh, dg).start()
            copy_d(i, dh).start()

    def relay_group(i):
        for dh in range(1, highs):
            for dg in range(1, groups):
                copy_c(i, dh, dg).wait_recv()
                copy_e(i, dh, dg).start()

    def arrived(i):
        copy_a(i).wait_recv()
        for dh in range(1, highs):
            copy_d(i, dh).wait_recv()
            for dg in range(1, groups):
                copy_e(i, dh, dg).wait_recv()

    halo_copy = remote(
        conv_hbm.at[pl.ds(rows - halo, halo)],
        ext.at[pl.ds(0, halo)],
        sem_halo,
        (0,),
        {"ep": (e + 1) % eps},
    )

    @pl.when(e < eps - 1)
    def _():
        halo_copy.start()

    @pl.when(e == 0)
    def _():
        ext[0:halo, :] = jnp.zeros((halo, width), BF16)

    ids = ids_ref[pl.ds(pl.multiple_of(t * block, 8), block), :]
    weights = route_ref[pl.ds(pl.multiple_of(t * block, 8), block), :]
    lane = lax.broadcasted_iota(jnp.int32, (block, LANES), 1)
    below = (
        lax.broadcasted_iota(jnp.int32, (block, block), 0)
        > lax.broadcasted_iota(jnp.int32, (block, block), 1)
    )
    below = jnp.where(below, 1.0, 0.0).astype(BF16)
    slot = lax.broadcasted_iota(jnp.int32, (block, slots), 1).astype(F32)
    seen = jnp.zeros((1, LANES), F32)
    pick = jnp.zeros((block, slots), F32)
    mixing = jnp.zeros((block, slots), F32)
    for k in range(2):
        named = ids[:, k : k + 1]
        onehot = jnp.where(named == lane, 1.0, 0.0)
        before = jnp.dot(below, onehot.astype(BF16), preferred_element_type=F32) + seen
        position = jnp.sum(before * onehot, axis=1, keepdims=True)
        seen = seen + jnp.sum(onehot, axis=0, keepdims=True)
        target = named.astype(F32) * float(cap) + position
        here = jnp.where(target == slot, 1.0, 0.0)
        pick = pick + here
        mixing = mixing + here * weights[:, k : k + 1]
    mix_high = mixing.astype(BF16)
    mix[0] = mix_high
    mix[1] = (mixing - mix_high.astype(F32)).astype(BF16)

    local[0].wait()
    own = own_in[...].astype(F32)
    scale = lax.rsqrt(jnp.mean(own * own, axis=1, keepdims=True) + EPSILON)
    normed = (own * scale * moe_gain[...]).astype(BF16)
    chosen = lax.dot_general(
        pick.astype(BF16), normed, (((0,), (0,)), ((), ())), preferred_element_type=F32
    ).astype(BF16)
    send_rows[...] = chosen.reshape(eps, cap, width)

    def copy_x(de):
        other = (e + de) % eps
        return remote(send_rows.at[other], got_rows.at[e], sem_x, (de,), {"ep": other})

    def copy_y(de, part):
        other = (e + de) % eps
        columns = pl.ds(part * half, half)
        return remote(
            result.at[other, :, columns],
            back.at[e, :, columns],
            sem_y,
            (de, part),
            {"ep": other},
        )

    for de in range(1, eps):
        copy_x(de).start()
    got_rows[pl.ds(e, 1)] = send_rows[pl.ds(e, 1)]

    local[1].wait()

    def conv_chunk(j):
        row0 = pl.multiple_of(j * CONV_ROWS, CONV_ROWS)
        tall = CONV_ROWS + halo

        def columns_of(c):
            return pl.ds(pl.multiple_of(c * LANES, LANES), LANES)

        def first(c, squares):
            columns = columns_of(c)
            window = ext[pl.ds(row0, tall), columns].astype(F32)
            total = jnp.zeros((CONV_ROWS, LANES), F32)
            for phase in range(8):
                shifts = [k for k in range(halo - reach, halo + 1) if k % 8 == phase]
                top = max(shifts) - phase
                shifted = window[phase : phase + top + CONV_ROWS]
                for k in shifts:
                    tap = taps[pl.ds(k - halo + reach, 1), columns]
                    total = total + shifted[k - phase : k - phase + CONV_ROWS] * tap
            conv_sum[:, columns] = total
            return squares + total * total

        squares = lax.fori_loop(0, width // LANES, first, jnp.zeros((CONV_ROWS, LANES), F32))
        mean = jnp.sum(squares, axis=1, keepdims=True) * (1.0 / width)
        rate = lax.rsqrt(mean + EPSILON)

        def second(c, carry):
            columns = columns_of(c)
            value = conv_sum[:, columns] * rate * conv_gain[:, columns]
            act[pl.ds(row0, CONV_ROWS), columns] = silu(value).astype(BF16)
            return carry

        lax.fori_loop(0, width // LANES, second, 0)

    chunks = rows // CONV_ROWS

    def conv_range(start, stop):
        def step(j, carry):
            conv_chunk(j)
            return carry

        lax.fori_loop(start, stop, step, 0)

    cuts = [1 + (chunks - 1) * i // 4 for i in range(5)]
    conv_range(cuts[0], cuts[1])
    relay_cross(0)
    conv_range(cuts[1], cuts[2])
    relay_cross(1)
    relay_group(0)
    conv_range(cuts[2], cuts[3])
    relay_cross(2)
    relay_group(1)
    conv_range(cuts[3], cuts[4])

    @pl.when(e > 0)
    def _():
        halo_copy.wait_recv()

    conv_range(0, 1)
    relay_cross(3)
    relay_group(2)

    local[2].wait()
    out_rows = rows // 2

    def project(j, carry):
        where = pl.ds(pl.multiple_of(j * out_rows, 16), out_rows)
        conv_out[where, :] = jnp.dot(
            act[where, :], convw[...], preferred_element_type=F32
        ).astype(BF16)
        return carry

    lax.fori_loop(0, 2, project, 0)

    relay_cross(4)
    relay_group(3)
    for de in range(1, eps):
        copy_x(de).wait_recv()
    local[3].wait()
    arrived(0)
    arrived(1)

    def gates(q, carry):
        gate_val[q] = jnp.dot(
            got_rows[...].reshape(slots, width), gate[q], preferred_element_type=F32
        )
        return carry

    lax.fori_loop(0, tps, gates, 0)
    relay_cross(5)
    relay_group(4)
    local[4].wait()
    arrived(2)
    arrived(3)

    def ups(q, carry):
        value = jnp.dot(got_rows[...].reshape(slots, width), up[q], preferred_element_type=F32)
        hidden[q] = (silu(gate_val[q]) * value).astype(BF16)
        return carry

    lax.fori_loop(0, tps, ups, 0)
    local[5].wait()
    tile = 256
    for part in range(2):
        if part == 1:
            relay_group(5)
        arrived(4 + part)

        def downs(n, carry):
            columns = pl.ds(pl.multiple_of(part * half + n * tile, tile), tile)
            value = jnp.dot(hidden[0], down[0, :, columns], preferred_element_type=F32)
            for q in range(1, tps):
                value = value + jnp.dot(hidden[q], down[q, :, columns], preferred_element_type=F32)
            result[:, :, columns] = value.astype(BF16).reshape(eps, cap, tile)
            return carry

        lax.fori_loop(0, half // tile, downs, 0)
        for de in range(1, eps):
            copy_y(de, part).start()
    back[pl.ds(e, 1)] = result[pl.ds(e, 1)]
    for de in range(1, eps):
        for part in range(2):
            copy_y(de, part).wait_recv()
    every = back[...].reshape(slots, width)
    mixed = jnp.dot(mix[0], every, preferred_element_type=F32) + jnp.dot(
        mix[1], every, preferred_element_type=F32
    )
    scale = lax.rsqrt(jnp.mean(mixed * mixed, axis=1, keepdims=True) + EPSILON)
    moe_out[...] = (mixed * scale * post_gain[...]).astype(BF16)

    @pl.when(e < eps - 1)
    def _():
        halo_copy.wait_send()

    for i in range(count):
        copy_a(i).wait_send()
        for dh in range(1, highs):
            copy_b(i, dh).wait_send()
            copy_d(i, dh).wait_send()
            for dg in range(1, groups):
                copy_c(i, dh, dg).wait_send()
                copy_e(i, dh, dg).wait_send()
    for de in range(1, eps):
        copy_x(de).wait_send()
        for part in range(2):
            copy_y(de, part).wait_send()


def body(
    sizes,
    conv_input,
    conv_taps,
    conv_gain,
    conv_weight,
    moe_input,
    moe_gain,
    expert_ids,
    route_weights,
    gate_weight,
    up_weight,
    down_weight,
    post_gain,
):
    groups, eps, tps = sizes
    highs = tps // 2
    rows, width = conv_input.shape
    block = moe_input.shape[0] // tps
    cap = 2 * block // eps
    units = gate_weight.shape[2]
    halo = (conv_taps.shape[0] - 1 + 15) // 16 * 16
    vmem = pl.BlockSpec(memory_space=pltpu.VMEM)
    hbm = pl.BlockSpec(memory_space=pl.ANY)
    dma = pltpu.SemaphoreType.DMA
    items = 6
    call = pl.pallas_call(
        functools.partial(kernel, sizes),
        out_shape=(
            jax.ShapeDtypeStruct((rows, conv_weight.shape[1]), BF16),
            jax.ShapeDtypeStruct((block, width), BF16),
        ),
        in_specs=[hbm, vmem, vmem, hbm, hbm, vmem, vmem, vmem, hbm, hbm, hbm, vmem],
        out_specs=(vmem, vmem),
        scratch_shapes=[
            pltpu.VMEM((rows + halo, width), BF16),
            pltpu.VMEM(conv_weight.shape, BF16),
            pltpu.VMEM((rows, width), BF16),
            pltpu.VMEM((CONV_ROWS, width), F32),
            pltpu.VMEM((block, width), BF16),
            pltpu.VMEM((tps, width, units), BF16),
            pltpu.VMEM((tps, width, units), BF16),
            pltpu.VMEM((tps, units, width), BF16),
            pltpu.VMEM((2, block, 2 * block), BF16),
            pltpu.VMEM((eps, cap, width), BF16),
            pltpu.VMEM((eps, cap, width), BF16),
            pltpu.VMEM((tps, 2 * block, units), F32),
            pltpu.VMEM((tps, 2 * block, units), BF16),
            pltpu.VMEM((eps, cap, width), BF16),
            pltpu.VMEM((eps, cap, width), BF16),
            dma((6,)),
            dma((2, 1)),
            dma((2, items)),
            dma((2, items, highs)),
            dma((2, items, highs, groups)),
            dma((2, items, highs)),
            dma((2, items, highs, groups)),
            dma((2, eps)),
            dma((2, eps, 2)),
        ],
        compiler_params=pltpu.CompilerParams(
            collective_id=0, has_side_effects=True, vmem_limit_bytes=60 * 1024 * 1024
        ),
    )
    return call(
        conv_input,
        conv_taps,
        conv_gain.reshape(1, width),
        conv_weight,
        moe_input,
        moe_gain.reshape(1, width),
        expert_ids,
        route_weights,
        gate_weight,
        up_weight,
        down_weight,
        post_gain.reshape(1, width),
    )


def solution(mesh):
    in_specs = (
        P(("grp", "ep"), None),
        P(),
        P(),
        P(None, "tp"),
        P(("grp", "ep"), None),
        P(),
        P(("grp", "ep"), None),
        P(("grp", "ep"), None),
        P("ep", None, "tp"),
        P("ep", None, "tp"),
        P("ep", "tp", None),
        P(),
    )
    out_specs = (P(("grp", "ep"), "tp"), P(("grp", "ep", "tp"), None))
    sizes = (mesh.shape["grp"], mesh.shape["ep"], mesh.shape["tp"])
    return jax.shard_map(
        functools.partial(body, sizes),
        mesh=mesh,
        in_specs=in_specs,
        out_specs=out_specs,
        check_vma=False,
    )
```

time: 227 us -> 97.8 us (0.43)
  other arithmetic: 96 us -> 0 us
  Pallas kernels: 0 us -> 88.6 us
  waiting for transfers between devices: 55.3 us -> 0 us
  local copies, waits for them, and re-layouts: 27.4 us -> 7.13 us
  matrix products: 17.4 us -> 0 us
  starting transfers between devices: 15.6 us -> 0 us
  between operations: 14 us -> 0.64 us
    pallas_call x0 -> x1, Pallas kernels: none -> 88.6 us  [body(): call(conv_input, conv_taps, conv_gain.reshape(1, width), conv_weight, moe...]
    reduce_sum x5 -> x0, other arithmetic: 80.1 us -> none  [the longest x3 74.2 us: channel_norm(): mean_square = jnp.mean(values * values, axis=-1, keepdims=True)]
    all_gather x3 -> x0, waiting for transfers between devices: 40.8 us -> none  [the longest x1 29.2 us: body(): lax.all_gather(down_weight, 'tp', axis=1, tiled=True)]
    dot_general x4 -> x0, matrix products: 17.4 us -> none  [the longest x1 5.12 us: body(): jnp.einsum('sjctf,jtfd->sjctd', pieces, down_pieces, preferred_element_ty...]
    all_to_all x2 -> x0, starting transfers between devices: 10.9 us -> none  [the longest x1 6.34 us: body(): lax.all_to_all(normed[own_source // 2].reshape(1, ep_count, local_experts...]
    ppermute x1 -> x0, waiting for transfers between devices: 10.2 us -> none  [shifted(): return lax.ppermute(shard, axis, pairs)]
    convert_element_type x3 -> x0, other arithmetic: 7.35 us -> none  [the longest x1 5.01 us: body(): jnp.concatenate([carried, conv_input], axis=0).astype(jnp.float32)]
    slice x5 -> x0, local copies, waits for them, and re-layouts: 6.21 us -> none  [the longest x1 2.37 us: body(): conv_sum = extended[0:row_count] * conv_taps[0]]
  transfers between devices with their start and end apart: 6 -> 0, of which waited for: 4 -> 0; matrix products, arithmetic and copies ran while one was open for 54% -> 0% of each run, Pallas kernels for 0% -> 0%
where the time goes in v1:
time: 97.8 us; the launch traced here: 96.3 us
  Pallas kernels  88.6 us (91%)
  local copies, waits for them, and re-layouts  7.13 us (7%)
    pallas_call x1, Pallas kernels, body(): call(conv_input, conv_taps, conv_gain.reshape(1, width), conv_weight, moe...  88.6 us
    unnamed x4, local copies, waits for them, and re-layouts  7.13 us

profile of v1, /device:TPU:0, one launch (start us, length us, event | category | flops | bytes accessed | tf_op | source)
XLA Modules:
  0.0 96.3 jit_solution(18284403247080429006)
XLA Ops:
  0.6 1.6 %copy.14.ids_ref = s32[640,2]{1,0:T(8,128)} copy(s32[640,2]{0,1:T(2,128)} %param.18) | data formatting | bytes 10240 | tf_op args[6]
  2.2 1.6 %copy.15.route_ref = f32[640,2]{1,0:T(8,128)} copy(f32[640,2]{0,1:T(2,128)} %param.19) | data formatting | bytes 10240 | tf_op args[7]
  3.8 88.6 %shard_map.131 = (bf16[640,512]{1,0:T(8,128)(2,1)}, bf16[160,2048]{1,0:T(8,128)(2,1)}) custom-call(bf16[640,2048]{1,0:T(8,128)(2,1)} %conv_hbm.1, f32[31,2048]{1,0:T(8,128)} %taps.1, f32[1,2048]{1,0:T(1,128)} %bitcast.3, bf16[2048,512]{1,0:T(8,128)(2,1)} %convw_hbm.1, bf16[640,2048]{1,0:T(8,128)(2,1)} %moe_hbm.1, f32[1,2048]{1,0:T(1,128)} %bitcast.4, ...), custom_call_target="tpu_custom_call" | custom-call | tf_op jit(solution)/shard_map/pallas_call | solution.py:465
  92.4 2.0 %copy.18 = bf16[640,512]{1,0:T(8,128)(2,1)} copy(bf16[640,512]{1,0:T(8,128)(2,1)} %get-tuple-element.4) | data formatting | bytes 1310720
  94.4 2.0 %copy.19 = bf16[160,2048]{1,0:T(8,128)(2,1)} copy(bf16[160,2048]{1,0:T(8,128)(2,1)} %get-tuple-element.5) | data formatting | bytes 1310720

commit v2 on v1

--- a/solution.py
+++ b/solution.py
@@ -12,6 +12,7 @@
 F32, BF16 = jnp.float32, jnp.bfloat16
 CONV_ROWS = 64
 LANES = 128
+EARLY = 7
 
 
 def silu(v):
@@ -110,8 +111,10 @@
     for source, buffer in ((gate_hbm, gate), (up_hbm, up)):
         for part in range(2):
             items.append((source, buffer, part * half, half, 0, units))
-    for part in range(2):
-        items.append((down_hbm, down, 0, units, part * half, half))
+    parts = 4
+    slab = width // parts
+    for part in range(parts):
+        items.append((down_hbm, down, 0, units, part * slab, slab))
 
     def view(ref, item, piece=None):
         _, _, r0, count, c0, columns = item
@@ -195,28 +198,33 @@
     def _():
         ext[0:halo, :] = jnp.zeros((halo, width), BF16)
 
-    ids = ids_ref[pl.ds(pl.multiple_of(t * block, 8), block), :]
-    weights = route_ref[pl.ds(pl.multiple_of(t * block, 8), block), :]
-    lane = lax.broadcasted_iota(jnp.int32, (block, LANES), 1)
-    below = (
+    ids = jnp.zeros((2, block), jnp.int32)
+    weights = jnp.zeros((2, block), F32)
+    for q in range(tps):
+        span = slice(q * block, (q + 1) * block)
+        ids = jnp.where(t == q, ids_ref[:, span], ids)
+        weights = jnp.where(t == q, route_ref[:, span], weights)
+    experts = max(8, eps)
+    kind = lax.broadcasted_iota(jnp.int32, (experts, block), 0)
+    above = (
         lax.broadcasted_iota(jnp.int32, (block, block), 0)
-        > lax.broadcasted_iota(jnp.int32, (block, block), 1)
+        < lax.broadcasted_iota(jnp.int32, (block, block), 1)
     )
-    below = jnp.where(below, 1.0, 0.0).astype(BF16)
-    slot = lax.broadcasted_iota(jnp.int32, (block, slots), 1).astype(F32)
-    seen = jnp.zeros((1, LANES), F32)
-    pick = jnp.zeros((block, slots), F32)
-    mixing = jnp.zeros((block, slots), F32)
+    above = jnp.where(above, 1.0, 0.0).astype(BF16)
+    slot = lax.broadcasted_iota(jnp.int32, (slots, block), 0).astype(F32)
+    seen = jnp.zeros((experts, 1), F32)
+    pick = jnp.zeros((slots, block), F32)
+    mixing = jnp.zeros((slots, block), F32)
     for k in range(2):
-        named = ids[:, k : k + 1]
-        onehot = jnp.where(named == lane, 1.0, 0.0)
-        before = jnp.dot(below, onehot.astype(BF16), preferred_element_type=F32) + seen
-        position = jnp.sum(before * onehot, axis=1, keepdims=True)
-        seen = seen + jnp.sum(onehot, axis=0, keepdims=True)
+        named = ids[k : k + 1, :]
+        onehot = jnp.where(named == kind, 1.0, 0.0)
+        before = jnp.dot(onehot.astype(BF16), above, preferred_element_type=F32) + seen
+        position = jnp.sum(before * onehot, axis=0, keepdims=True)
+        seen = seen + jnp.sum(onehot, axis=1, keepdims=True)
         target = named.astype(F32) * float(cap) + position
         here = jnp.where(target == slot, 1.0, 0.0)
         pick = pick + here
-        mixing = mixing + here * weights[:, k : k + 1]
+        mixing = mixing + here * weights[k : k + 1, :]
     mix_high = mixing.astype(BF16)
     mix[0] = mix_high
     mix[1] = (mixing - mix_high.astype(F32)).astype(BF16)
@@ -225,9 +233,7 @@
     own = own_in[...].astype(F32)
     scale = lax.rsqrt(jnp.mean(own * own, axis=1, keepdims=True) + EPSILON)
     normed = (own * scale * moe_gain[...]).astype(BF16)
-    chosen = lax.dot_general(
-        pick.astype(BF16), normed, (((0,), (0,)), ((), ())), preferred_element_type=F32
-    ).astype(BF16)
+    chosen = jnp.dot(pick.astype(BF16), normed, preferred_element_type=F32).astype(BF16)
     send_rows[...] = chosen.reshape(eps, cap, width)
 
     def copy_x(de):
@@ -236,7 +242,7 @@
 
     def copy_y(de, part):
         other = (e + de) % eps
-        columns = pl.ds(part * half, half)
+        columns = pl.ds(part * slab, slab)
         return remote(
             result.at[other, :, columns],
             back.at[e, :, columns],
@@ -293,25 +299,73 @@
 
         lax.fori_loop(start, stop, step, 0)
 
-    cuts = [1 + (chunks - 1) * i // 4 for i in range(5)]
-    conv_range(cuts[0], cuts[1])
+    conv_range(1, 2)
     relay_cross(0)
-    conv_range(cuts[1], cuts[2])
+    conv_range(2, 3)
     relay_cross(1)
+    conv_range(3, 4)
     relay_group(0)
-    conv_range(cuts[2], cuts[3])
+    conv_range(4, 5)
     relay_cross(2)
     relay_group(1)
-    conv_range(cuts[3], cuts[4])
+    conv_range(5, 6)
+    relay_cross(3)
+    conv_range(6, EARLY)
+    relay_group(2)
+    relay_cross(4)
+    relay_cross(5)
+    for de in range(1, eps):
+        copy_x(de).wait_recv()
+    local[3].wait()
+    arrived(0)
+    arrived(1)
+
+    def gates(q, carry):
+        gate_val[q] = jnp.dot(
+            got_rows[...].reshape(slots, width), gate[q], preferred_element_type=F32
+        )
+        return carry
+
+    lax.fori_loop(0, tps, gates, 0)
+    relay_group(3)
+    relay_cross(6)
+    relay_cross(7)
+    local[4].wait()
+    arrived(2)
+    arrived(3)
+
+    def ups(q, carry):
+        value = jnp.dot(got_rows[...].reshape(slots, width), up[q], preferred_element_type=F32)
+        hidden[q] = (silu(gate_val[q]) * value).astype(BF16)
+        return carry
+
+    lax.fori_loop(0, tps, ups, 0)
+    local[5].wait()
+    tile = 256
+    for part in range(parts):
+        relay_group(4 + part)
+        arrived(4 + part)
+
+        def downs(n, carry):
+            columns = pl.ds(pl.multiple_of(part * slab + n * tile, tile), tile)
+            value = jnp.dot(hidden[0], down[0, :, columns], preferred_element_type=F32)
+            for q in range(1, tps):
+                value = value + jnp.dot(hidden[q], down[q, :, columns], preferred_element_type=F32)
+            result[:, :, columns] = value.astype(BF16).reshape(eps, cap, tile)
+            return carry
+
+        lax.fori_loop(0, slab // tile, downs, 0)
+        for de in range(1, eps):
+            copy_y(de, part).start()
+    back[pl.ds(e, 1)] = result[pl.ds(e, 1)]
+
+    conv_range(EARLY, chunks)
 
     @pl.when(e > 0)
     def _():
         halo_copy.wait_recv()
 
     conv_range(0, 1)
-    relay_cross(3)
-    relay_group(2)
-
     local[2].wait()
     out_rows = rows // 2
 
@@ -323,60 +377,13 @@
         return carry
 
     lax.fori_loop(0, 2, project, 0)
-
-    relay_cross(4)
-    relay_group(3)
-    for de in range(1, eps):
-        copy_x(de).wait_recv()
-    local[3].wait()
-    arrived(0)
-    arrived(1)
-
-    def gates(q, carry):
-        gate_val[q] = jnp.dot(
-            got_rows[...].reshape(slots, width), gate[q], preferred_element_type=F32
-        )
-        return carry
-
-    lax.fori_loop(0, tps, gates, 0)
-    relay_cross(5)
-    relay_group(4)
-    local[4].wait()
-    arrived(2)
-    arrived(3)
-
-    def ups(q, carry):
-        value = jnp.dot(got_rows[...].reshape(slots, width), up[q], preferred_element_type=F32)
-        hidden[q] = (silu(gate_val[q]) * value).astype(BF16)
-        return carry
-
-    lax.fori_loop(0, tps, ups, 0)
-    local[5].wait()
-    tile = 256
-    for part in range(2):
-        if part == 1:
-            relay_group(5)
-        arrived(4 + part)
-
-        def downs(n, carry):
-            columns = pl.ds(pl.multiple_of(part * half + n * tile, tile), tile)
-            value = jnp.dot(hidden[0], down[0, :, columns], preferred_element_type=F32)
-            for q in range(1, tps):
-                value = value + jnp.dot(hidden[q], down[q, :, columns], preferred_element_type=F32)
-            result[:, :, columns] = value.astype(BF16).reshape(eps, cap, tile)
-            return carry
-
-        lax.fori_loop(0, half // tile, downs, 0)
+    for part in range(parts):
         for de in range(1, eps):
-            copy_y(de, part).start()
-    back[pl.ds(e, 1)] = result[pl.ds(e, 1)]
-    for de in range(1, eps):
-        for part in range(2):
             copy_y(de, part).wait_recv()
     every = back[...].reshape(slots, width)
-    mixed = jnp.dot(mix[0], every, preferred_element_type=F32) + jnp.dot(
-        mix[1], every, preferred_element_type=F32
-    )
+    turned = (((0,), (0,)), ((), ()))
+    mixed = lax.dot_general(mix[0], every, turned, preferred_element_type=F32)
+    mixed = mixed + lax.dot_general(mix[1], every, turned, preferred_element_type=F32)
     scale = lax.rsqrt(jnp.mean(mixed * mixed, axis=1, keepdims=True) + EPSILON)
     moe_out[...] = (mixed * scale * post_gain[...]).astype(BF16)
 
@@ -394,7 +401,7 @@
                 copy_e(i, dh, dg).wait_send()
     for de in range(1, eps):
         copy_x(de).wait_send()
-        for part in range(2):
+        for part in range(parts):
             copy_y(de, part).wait_send()
 
 
@@ -423,7 +430,7 @@
     vmem = pl.BlockSpec(memory_space=pltpu.VMEM)
     hbm = pl.BlockSpec(memory_space=pl.ANY)
     dma = pltpu.SemaphoreType.DMA
-    items = 6
+    items = 8
     call = pl.pallas_call(
         functools.partial(kernel, sizes),
         out_shape=(
@@ -441,7 +448,7 @@
             pltpu.VMEM((tps, width, units), BF16),
             pltpu.VMEM((tps, width, units), BF16),
             pltpu.VMEM((tps, units, width), BF16),
-            pltpu.VMEM((2, block, 2 * block), BF16),
+            pltpu.VMEM((2, 2 * block, block), BF16),
             pltpu.VMEM((eps, cap, width), BF16),
             pltpu.VMEM((eps, cap, width), BF16),
             pltpu.VMEM((tps, 2 * block, units), F32),
@@ -456,7 +463,7 @@
             dma((2, items, highs)),
             dma((2, items, highs, groups)),
             dma((2, eps)),
-            dma((2, eps, 2)),
+            dma((2, eps, 4)),
         ],
         compiler_params=pltpu.CompilerParams(
             collective_id=0, has_side_effects=True, vmem_limit_bytes=60 * 1024 * 1024
@@ -469,8 +476,8 @@
         conv_weight,
         moe_input,
         moe_gain.reshape(1, width),
-        expert_ids,
-        route_weights,
+        expert_ids.T,
+        route_weights.T,
         gate_weight,
         up_weight,
         down_weight,

time: 97.8 us -> 83.4 us (0.85); the launches traced: 96.3 us -> 83.2 us
  Pallas kernels: 88.6 us -> 78.6 us
  local copies, waits for them, and re-layouts: 7.13 us -> 3.95 us
    pallas_call x1, Pallas kernels: 88.6 us -> 78.6 us  [body(): call(conv_input, conv_taps, conv_gain.reshape(1, width), conv_weight, moe...]
    unnamed x4 -> x2, local copies, waits for them, and re-layouts: 7.13 us -> 3.95 us
where the time goes in v2:
time: 83.4 us; the launch traced here: 83.2 us
  Pallas kernels  78.6 us (94%)
  local copies, waits for them, and re-layouts  3.95 us (5%)
    pallas_call x1, Pallas kernels, body(): call(conv_input, conv_taps, conv_gain.reshape(1, width), conv_weight, moe...  78.6 us
    unnamed x2, local copies, waits for them, and re-layouts  3.95 us

profile of v2, /device:TPU:0, one launch (start us, length us, event | category | flops | bytes accessed | tf_op | source)
XLA Modules:
  0.0 83.2 jit_solution(8409009043598615183)
XLA Ops:
  0.6 78.6 %shard_map.131 = (bf16[640,512]{1,0:T(8,128)(2,1)}, bf16[160,2048]{1,0:T(8,128)(2,1)}) custom-call(bf16[640,2048]{1,0:T(8,128)(2,1)} %conv_hbm.1, f32[31,2048]{1,0:T(8,128)} %taps.1, f32[1,2048]{1,0:T(1,128)} %bitcast.5, bf16[2048,512]{1,0:T(8,128)(2,1)} %convw_hbm.1, bf16[640,2048]{1,0:T(8,128)(2,1)} %moe_hbm.1, f32[1,2048]{1,0:T(1,128)} %bitcast.6, ...), custom_call_target="tpu_custom_call" | custom-call | tf_op jit(solution)/shard_map/pallas_call | solution.py:472
  79.2 2.0 %copy.16 = bf16[640,512]{1,0:T(8,128)(2,1)} copy(bf16[640,512]{1,0:T(8,128)(2,1)} %get-tuple-element.4) | data formatting | bytes 1310720
  81.2 2.0 %copy.17 = bf16[160,2048]{1,0:T(8,128)(2,1)} copy(bf16[160,2048]{1,0:T(8,128)(2,1)} %get-tuple-element.5) | data formatting | bytes 1310720

commit v3 on v2

--- a/solution.py
+++ b/solution.py
@@ -12,7 +12,8 @@
 F32, BF16 = jnp.float32, jnp.bfloat16
 CONV_ROWS = 64
 LANES = 128
-EARLY = 7
+PARTS = 4
+PAIR = 2
 
 
 def silu(v):
@@ -39,6 +40,7 @@
     convw,
     act,
     conv_sum,
+    window,
     own_in,
     gate,
     up,
@@ -107,12 +109,11 @@
         )
 
     items = []
-    half = width // 2
+    parts = PARTS
+    slab = width // parts
     for source, buffer in ((gate_hbm, gate), (up_hbm, up)):
-        for part in range(2):
-            items.append((source, buffer, part * half, half, 0, units))
-    parts = 4
-    slab = width // parts
+        for part in range(parts):
+            items.append((source, buffer, part * slab, slab, 0, units))
     for part in range(parts):
         items.append((down_hbm, down, 0, units, part * slab, slab))
 
@@ -264,21 +265,22 @@
         def columns_of(c):
             return pl.ds(pl.multiple_of(c * LANES, LANES), LANES)
 
-        def first(c, squares):
-            columns = columns_of(c)
-            window = ext[pl.ds(row0, tall), columns].astype(F32)
-            total = jnp.zeros((CONV_ROWS, LANES), F32)
-            for phase in range(8):
-                shifts = [k for k in range(halo - reach, halo + 1) if k % 8 == phase]
-                top = max(shifts) - phase
-                shifted = window[phase : phase + top + CONV_ROWS]
-                for k in shifts:
-                    tap = taps[pl.ds(k - halo + reach, 1), columns]
-                    total = total + shifted[k - phase : k - phase + CONV_ROWS] * tap
-            conv_sum[:, columns] = total
-            return squares + total * total
-
-        squares = lax.fori_loop(0, width // LANES, first, jnp.zeros((CONV_ROWS, LANES), F32))
+        def first(pair, squares):
+            for side in range(PAIR):
+                columns = columns_of(pair * PAIR + side)
+                window[side] = ext[pl.ds(row0, tall), columns].astype(F32)
+            for side in range(PAIR):
+                columns = columns_of(pair * PAIR + side)
+                total = jnp.zeros((CONV_ROWS, LANES), F32)
+                for k in range(reach + 1):
+                    shifted = window[side, pl.ds(halo - reach + k, CONV_ROWS), :]
+                    total = total + shifted * taps[pl.ds(k, 1), columns]
+                conv_sum[:, columns] = total
+                squares = squares + total * total
+            return squares
+
+        start = jnp.zeros((CONV_ROWS, LANES), F32)
+        squares = lax.fori_loop(0, width // LANES // PAIR, first, start)
         mean = jnp.sum(squares, axis=1, keepdims=True) * (1.0 / width)
         rate = lax.rsqrt(mean + EPSILON)
 
@@ -299,26 +301,22 @@
 
         lax.fori_loop(start, stop, step, 0)
 
-    conv_range(1, 2)
-    relay_cross(0)
-    conv_range(2, 3)
-    relay_cross(1)
-    conv_range(3, 4)
-    relay_group(0)
-    conv_range(4, 5)
-    relay_cross(2)
-    relay_group(1)
-    conv_range(5, 6)
-    relay_cross(3)
-    conv_range(6, EARLY)
-    relay_group(2)
-    relay_cross(4)
-    relay_cross(5)
+    def step(i):
+        relay_cross(i)
+        if i > 0:
+            relay_group(i - 1)
+
+    early = min(chunks, 2 * parts + 1)
+    for i in range(2 * parts):
+        if 1 + i < early:
+            conv_range(1 + i, 2 + i)
+        step(i)
+    step(2 * parts)
     for de in range(1, eps):
         copy_x(de).wait_recv()
     local[3].wait()
-    arrived(0)
-    arrived(1)
+    for i in range(parts):
+        arrived(i)
 
     def gates(q, carry):
         gate_val[q] = jnp.dot(
@@ -327,12 +325,10 @@
         return carry
 
     lax.fori_loop(0, tps, gates, 0)
-    relay_group(3)
-    relay_cross(6)
-    relay_cross(7)
+    step(2 * parts + 1)
     local[4].wait()
-    arrived(2)
-    arrived(3)
+    for i in range(parts):
+        arrived(parts + i)
 
     def ups(q, carry):
         value = jnp.dot(got_rows[...].reshape(slots, width), up[q], preferred_element_type=F32)
@@ -343,8 +339,9 @@
     local[5].wait()
     tile = 256
     for part in range(parts):
-        relay_group(4 + part)
-        arrived(4 + part)
+        if part + 1 == parts:
+            relay_group(count - 1)
+        arrived(2 * parts + part)
 
         def downs(n, carry):
             columns = pl.ds(pl.multiple_of(part * slab + n * tile, tile), tile)
@@ -357,9 +354,12 @@
         lax.fori_loop(0, slab // tile, downs, 0)
         for de in range(1, eps):
             copy_y(de, part).start()
+        if part + 2 < parts:
+            step(2 * parts + 2 + part)
     back[pl.ds(e, 1)] = result[pl.ds(e, 1)]
 
-    conv_range(EARLY, chunks)
+    if early < chunks:
+        conv_range(early, chunks)
 
     @pl.when(e > 0)
     def _():
@@ -430,7 +430,7 @@
     vmem = pl.BlockSpec(memory_space=pltpu.VMEM)
     hbm = pl.BlockSpec(memory_space=pl.ANY)
     dma = pltpu.SemaphoreType.DMA
-    items = 8
+    items = 3 * PARTS
     call = pl.pallas_call(
         functools.partial(kernel, sizes),
         out_shape=(
@@ -444,6 +444,7 @@
             pltpu.VMEM(conv_weight.shape, BF16),
             pltpu.VMEM((rows, width), BF16),
             pltpu.VMEM((CONV_ROWS, width), F32),
+            pltpu.VMEM((PAIR, CONV_ROWS + halo, LANES), F32),
             pltpu.VMEM((block, width), BF16),
             pltpu.VMEM((tps, width, units), BF16),
             pltpu.VMEM((tps, width, units), BF16),
@@ -463,7 +464,7 @@
             dma((2, items, highs)),
             dma((2, items, highs, groups)),
             dma((2, eps)),
-            dma((2, eps, 4)),
+            dma((2, eps, PARTS)),
         ],
         compiler_params=pltpu.CompilerParams(
             collective_id=0, has_side_effects=True, vmem_limit_bytes=60 * 1024 * 1024

time: 83.4 us -> 82.4 us (0.988)
  Pallas kernels: 78.6 us -> 77.6 us
    pallas_call x1, Pallas kernels: 78.6 us -> 77.6 us  [body(): call(conv_input, conv_taps, conv_gain.reshape(1, width), conv_weight, moe...]
where the time goes in v3:
time: 82.4 us; the launch traced here: 82.2 us
  Pallas kernels  77.6 us (94%)
  local copies, waits for them, and re-layouts  3.95 us (5%)
    pallas_call x1, Pallas kernels, body(): call(conv_input, conv_taps, conv_gain.reshape(1, width), conv_weight, moe...  77.6 us
    unnamed x2, local copies, waits for them, and re-layouts  3.95 us

profile of v3, /device:TPU:0, one launch (start us, length us, event | category | flops | bytes accessed | tf_op | source)
XLA Modules:
  0.0 82.2 jit_solution(2834011236885688882)
XLA Ops:
  0.6 77.6 %shard_map.131 = (bf16[640,512]{1,0:T(8,128)(2,1)}, bf16[160,2048]{1,0:T(8,128)(2,1)}) custom-call(bf16[640,2048]{1,0:T(8,128)(2,1)} %conv_hbm.1, f32[31,2048]{1,0:T(8,128)} %taps.1, f32[1,2048]{1,0:T(1,128)} %bitcast.5, bf16[2048,512]{1,0:T(8,128)(2,1)} %convw_hbm.1, bf16[640,2048]{1,0:T(8,128)(2,1)} %moe_hbm.1, f32[1,2048]{1,0:T(1,128)} %bitcast.6, ...), custom_call_target="tpu_custom_call" | custom-call | tf_op jit(solution)/shard_map/pallas_call | solution.py:473
  78.2 2.0 %copy.16 = bf16[640,512]{1,0:T(8,128)(2,1)} copy(bf16[640,512]{1,0:T(8,128)(2,1)} %get-tuple-element.4) | data formatting | bytes 1310720
  80.2 2.0 %copy.17 = bf16[160,2048]{1,0:T(8,128)(2,1)} copy(bf16[160,2048]{1,0:T(8,128)(2,1)} %get-tuple-element.5) | data formatting | bytes 1310720

commit v4 on v3

--- a/solution.py
+++ b/solution.py
@@ -470,7 +470,7 @@
             collective_id=0, has_side_effects=True, vmem_limit_bytes=60 * 1024 * 1024
         ),
     )
-    return call(
+    conv_part, moe_part = call(
         conv_input,
         conv_taps,
         conv_gain.reshape(1, width),
@@ -484,6 +484,21 @@
         down_weight,
         post_gain.reshape(1, width),
     )
+    return pl.pallas_call(
+        finish,
+        out_shape=(
+            jax.ShapeDtypeStruct(conv_part.shape, BF16),
+            jax.ShapeDtypeStruct(moe_part.shape, BF16),
+        ),
+        in_specs=[vmem, vmem],
+        out_specs=(vmem, vmem),
+        compiler_params=pltpu.CompilerParams(vmem_limit_bytes=16 * 1024 * 1024),
+    )(conv_part, moe_part)
+
+
+def finish(conv_part, moe_part, conv_out, moe_out):
+    conv_out[...] = conv_part[...]
+    moe_out[...] = moe_part[...]
 
 
 def solution(mesh):

time: 82.4 us -> 81.8 us (level)
  local copies, waits for them, and re-layouts: 3.95 us -> 2.17 us
  Pallas kernels: 77.6 us -> 78.7 us
    unnamed x2 -> x4, local copies, waits for them, and re-layouts: 3.95 us -> 2.17 us
    pallas_call x0 -> x1, Pallas kernels: none -> 1.14 us  [body(): pl.pallas_call(finish, out_shape=(jax.ShapeDtypeStruct(conv_part.shape, B...]
where the time goes in v4:
time: 81.8 us; the launch traced here: 81.5 us
  Pallas kernels  78.7 us (96%)
  local copies, waits for them, and re-layouts  2.17 us (3%)
    pallas_call x1, Pallas kernels, body(): call(conv_input, conv_taps, conv_gain.reshape(1, width), conv_weight, moe...  77.6 us
    unnamed x4, local copies, waits for them, and re-layouts  2.17 us

profile of v4, /device:TPU:0, one launch (start us, length us, event | category | flops | bytes accessed | tf_op | source)
XLA Modules:
  0.0 81.5 jit_solution(14224207580943272761)
XLA Ops:
  0.6 77.6 %shard_map.131 = (bf16[640,512]{1,0:T(8,128)(2,1)}, bf16[160,2048]{1,0:T(8,128)(2,1)}) custom-call(bf16[640,2048]{1,0:T(8,128)(2,1)} %conv_hbm.1, f32[31,2048]{1,0:T(8,128)} %taps.1, f32[1,2048]{1,0:T(1,128)} %bitcast.5, bf16[2048,512]{1,0:T(8,128)(2,1)} %convw_hbm.1, bf16[640,2048]{1,0:T(8,128)(2,1)} %moe_hbm.1, f32[1,2048]{1,0:T(1,128)} %bitcast.6, ...), custom_call_target="tpu_custom_call" | custom-call | tf_op jit(solution)/shard_map/pallas_call | solution.py:473
  78.2 0.0 copy-start
  78.2 1.1 %copy-done = bf16[640,512]{1,0:T(8,128)(2,1)S(1)} copy-done((bf16[640,512]{1,0:T(8,128)(2,1)S(1)}, bf16[640,512]{1,0:T(8,128)(2,1)}, u32[]{:S(2)}) %copy-start) | copy-done | bytes 655384
  79.3 0.0 copy-start.1
  79.3 1.1 %copy-done.1 = bf16[160,2048]{1,0:T(8,128)(2,1)S(1)} copy-done((bf16[160,2048]{1,0:T(8,128)(2,1)S(1)}, bf16[160,2048]{1,0:T(8,128)(2,1)}, u32[]{:S(2)}) %copy-start.1) | copy-done | bytes 655384
  80.4 1.1 %shard_map.132 = (bf16[640,512]{1,0:T(8,128)(2,1)}, bf16[160,2048]{1,0:T(8,128)(2,1)}) custom-call(bf16[640,512]{1,0:T(8,128)(2,1)S(1)} %copy-done, bf16[160,2048]{1,0:T(8,128)(2,1)S(1)} %copy-done.1), custom_call_target="tpu_custom_call" | custom-call | tf_op jit(solution)/shard_map/pallas_call | solution.py:487
Async XLA Ops:
  78.2 1.1 %copy-start = (bf16[640,512]{1,0:T(8,128)(2,1)S(1)}, bf16[640,512]{1,0:T(8,128)(2,1)}, u32[]{:S(2)}) copy-start(bf16[640,512]{1,0:T(8,128)(2,1)} %get-tuple-element.4.conv_part) | copy-start | bytes 1966084
  79.3 1.1 %copy-start.1 = (bf16[160,2048]{1,0:T(8,128)(2,1)S(1)}, bf16[160,2048]{1,0:T(8,128)(2,1)}, u32[]{:S(2)}) copy-start(bf16[160,2048]{1,0:T(8,128)(2,1)} %get-tuple-element.5.moe_part) | copy-start | bytes 1966084
